TPU v7x, 32 devices: a whole 2x2x4 slice. The times are simulated.
32 devices in a mesh: ep: 8 (over z, core), tp: 4 (over y, x).
Axes of the slice: x: 2, y: 2, z: 4, core: 2. Of those that a mesh axis runs over, the one named last changes fastest.
Arguments:
- value_in: bfloat16 [8192, 1536], P('ep', 'tp'), may hold values from -6 to 6
- gate_in: bfloat16 [8192, 1536], P('ep', 'tp'), may hold values from -9 to 9
- conv_kernel: float32 [31, 1536], P(None, 'tp'), may hold values from -40 to 40
- norm_gain: float32 [1536], replicated, may hold values from 0.1 to 1.9
- norm_shift: float32 [1536], replicated, may hold values from -3 to 3
- out_weight: bfloat16 [1536, 2048], P(None, 'tp'), may hold values from -0.15625 to 0.15625
- expert_input: bfloat16 [1536, 2048], P('ep'), may hold values from -6 to 6
- expert_gain: float32 [2048], replicated, may hold values from 0.1 to 1.9
- route_ids: int32 [1536, 4], P('ep'), may hold values from 0 to 7, all different within a row; in each aligned block of 192 rows (0 to 191, 192 to 383, ...) at most 120 rows name the same one
- route_weights: float32 [1536, 4], P('ep'), may hold values from 0.2 to 1
- gate_weight: bfloat16 [8, 2048, 2048], P('ep', None, 'tp'), may hold values from -0.375 to 0.375
- up_weight: bfloat16 [8, 2048, 2048], P('ep', None, 'tp'), may hold values from -0.375 to 0.375
- down_weight: bfloat16 [8, 2048, 2048], P('ep', None, 'tp'), may hold values from -0.01953125 to 0.01953125
Outputs:
- mixed_out: bfloat16 [8192, 2048], P('ep', 'tp')
- routed_out: bfloat16 [1536, 2048], P('ep', 'tp')
Inputs may be any that keep to these rules, and one draw needn't show every extreme that they name: `route_ids`: each row names 4 different experts; among the rows of one index of ep (aligned blocks of 192 rows) no expert is named by more than 120 rows, and in some block one expert is named by exactly 120.
All inputs are finite; a program needn't handle non-finite values.
Results may differ from a plain program's by a relative error of at most 0.0071.
Values may be sent and summed in bfloat16 or wider, within the bound.
A program may use at most 64 MiB of HBM per device.

v0:
```python
import jax
import jax.numpy as jnp
from jax import lax
from jax.sharding import PartitionSpec as P


def shifted(block, axis, distance):
    devices = range(lax.axis_size(axis))
    route = [(i - distance, i) for i in devices if i - distance in devices]
    return lax.ppermute(block, axis, route)


def expert_tail(gate_pre, up_pre, down_weight):
    clamped = jnp.minimum(gate_pre, 7.0)
    upward = jnp.clip(up_pre, -7.0, 7.0)
    activation = ((upward + 1.0) * clamped * jax.nn.sigmoid(1.702 * clamped)).astype(jnp.bfloat16)
    weights = down_weight[0]
    summed = jnp.dot(
        lax.all_gather(activation, "tp", axis=1, tiled=True),
        weights,
        preferred_element_type=jnp.float32,
    )
    return summed.astype(jnp.bfloat16)


def finish(gate_pre, up_pre, down_weight, arrived_shape):
    outcome = expert_tail(gate_pre, up_pre, down_weight)
    outcome = outcome.reshape(arrived_shape[0], arrived_shape[1], outcome.shape[1])
    return lax.all_to_all(outcome, "ep", split_axis=0, concat_axis=0, tiled=True)


def body(
    value_in,
    gate_in,
    conv_kernel,
    norm_gain,
    norm_shift,
    out_weight,
    expert_input,
    expert_gain,
    route_ids,
    route_weights,
    gate_weight,
    up_weight,
    down_weight,
):
    gated_values = (
        value_in.astype(jnp.float32) * jax.nn.sigmoid(gate_in.astype(jnp.float32))
    ).astype(jnp.bfloat16)
    kernel_width = conv_kernel.shape[0]
    length_dev = gated_values.shape[0]
    before = shifted(gated_values[length_dev - (kernel_width - 1) :], "ep", 1)
    extended = jnp.concatenate([before, gated_values], 0).astype(jnp.float32)
    running = jnp.zeros(gated_values.shape, jnp.float32)
    for tap_index in range(kernel_width):
        running = (
            running + conv_kernel[tap_index][None, :] * extended[tap_index : tap_index + length_dev]
        )
    convolved = running.astype(jnp.bfloat16)
    gathered = lax.all_gather(convolved, "tp", axis=1, tiled=True).astype(jnp.float32)
    row_mean = jnp.mean(gathered, axis=1, keepdims=True)
    row_var = jnp.mean(jnp.square(gathered - row_mean), axis=1, keepdims=True)
    normed = (gathered - row_mean) * lax.rsqrt(row_var + 1e-05) * norm_gain[None, :] + norm_shift[
        None, :
    ]
    hidden = jax.nn.silu(normed).astype(jnp.bfloat16)
    mixed_out = jnp.dot(hidden, out_weight, preferred_element_type=jnp.float32).astype(jnp.bfloat16)
    experts = lax.axis_size("ep")
    row_count, model_width = expert_input.shape
    top_count = route_ids.shape[1]
    capacity = (5 * row_count * top_count + 4 * experts - 1) // (4 * experts)
    input_float = expert_input.astype(jnp.float32)
    feature_mean = jnp.mean(input_float, axis=1, keepdims=True)
    feature_var = jnp.mean(jnp.square(input_float - feature_mean), axis=1, keepdims=True)
    normed_rows = (
        (input_float - feature_mean) * lax.rsqrt(feature_var + 1e-05) * expert_gain[None, :]
    ).astype(jnp.bfloat16)
    expert_ids = route_ids.reshape(-1)
    onehot = (expert_ids[:, None] == jnp.arange(experts, dtype=jnp.int32)[None, :]).astype(
        jnp.int32
    )
    earlier = jnp.cumsum(onehot, axis=0) - onehot
    position = jnp.sum(earlier * onehot, axis=1)
    destination = expert_ids * capacity + position
    token_index = jnp.arange(expert_ids.shape[0], dtype=jnp.int32) // top_count
    slot_token = (
        jnp.full((experts * capacity,), row_count, jnp.int32).at[destination].set(token_index)
    )
    padded = jnp.concatenate([normed_rows, jnp.zeros((1, model_width), jnp.bfloat16)], 0)
    outgoing = padded[slot_token].reshape(experts, capacity, model_width)
    column_width = model_width // lax.axis_size("tp")
    columns = lax.dynamic_slice_in_dim(
        outgoing, lax.axis_index("tp") * column_width, column_width, 2
    )
    arrived = lax.all_to_all(columns, "ep", split_axis=0, concat_axis=0, tiled=True)
    slot_total = arrived.shape[0] * arrived.shape[1]
    portion = lax.all_gather(arrived, "tp", axis=2, tiled=True)
    flattened = portion.reshape(slot_total, portion.shape[2])
    gate_part = gate_weight[0]
    up_part = up_weight[0]
    gate_pre = jnp.dot(flattened, gate_part, preferred_element_type=jnp.float32)
    up_pre = jnp.dot(flattened, up_part, preferred_element_type=jnp.float32)
    results_home = finish(gate_pre, up_pre, down_weight, arrived.shape)
    picked = results_home.reshape(-1, results_home.shape[2])[destination]
    picked = picked.reshape(row_count, top_count, -1).astype(jnp.float32)
    routed_out = jnp.sum(picked * route_weights[:, :, None], axis=1).astype(jnp.bfloat16)
    return (mixed_out, routed_out)


def solution(mesh):
    return jax.shard_map(
        body,
        mesh=mesh,
        in_specs=(
            P("ep", "tp"),
            P("ep", "tp"),
            P(None, "tp"),
            P(),
            P(),
            P(None, "tp"),
            P("ep", None),
            P(),
            P("ep", None),
            P("ep", None),
            P("ep", None, "tp"),
            P("ep", None, "tp"),
            P("ep", None, "tp"),
        ),
        out_specs=(P("ep", "tp"), P("ep", "tp")),
        check_vma=False,
    )
```

profile of v0, /device:TPU:0, one launch (start us, length us, event | category | flops | bytes accessed | tf_op | source)
XLA Modules:
  0.0 255.0 jit_solution(3363373219548088409)
XLA Ops:
  7.2 0.9 copy.19
  8.4 0.7 broadcast_multiply_fusion
  9.1 1.7 reduce-window.6
  10.9 0.1 copy.21
  11.1 0.2 reduce-window.9
  11.3 0.1 copy.18
  11.7 3.4 %scatter_custom_fusion = s32[960]{0:T(1024)S(1)} fusion(s32[768]{0:T(1024)S(1)} %fusion.69, s32[768]{0:T(1024)S(1)} %add_select_fusion, s32[]{:T(128)} %constant.28.clone.1), kind=kCustom, calls=%fused_computation.118 | custom fusion | bytes 3844 | tf_op jit(solution)/shard_map/scatter | solution.py:87
  15.1 1.3 convert_reduce_fusion.1
  16.4 0.4 fusion.23
  16.8 0.4 fusion.25
  17.3 5.9 %gather_fusion = bf16[960,2048]{1,0:T(8,128)(2,1)} fusion(bf16[193,2048]{1,0:T(8,128)(2,1)S(1)} %concatenate.7, s32[1024]{0:T(1024)S(1)} %pad_clamp_fusion.1), kind=kCustom, calls=%fused_computation | custom fusion | bytes 7868160 | tf_op jit(solution)/shard_map/gather | solution.py:90
  23.2 1.3 constant_dynamic-slice_fusion
  24.5 31.5 %all_to_all.10 = bf16[8,120,512]{2,1,0:T(8,128)(2,1)} all-to-all(bf16[8,120,512]{2,1,0:T(8,128)(2,1)S(1)} %constant_dynamic-slice_fusion), channel_id=1, replica_groups=mesh['ep'=8,'tp'=4] {'ep'}, dimensions={0} | all-to-all | bytes 1966080 | tf_op jit(solution)/shard_map/all_to_all | solution.py:95
  56.1 1.6 multiply_convert_fusion.1
  57.7 1.5 collective-permute-start
  59.4 0.6 collective-permute-done
  60.0 0.2 maximum_convert_fusion
  60.2 6.8 %fusion.27 = bf16[1024,384]{1,0:T(8,128)(2,1)} fusion(f32[1054,384]{1,0:T(8,128)S(1)} %maximum_convert_fusion, f32[384]{0:T(512)S(1)} %get-tuple-element.31, f32[384]{0:T(512)S(1)} %get-tuple-element.32, f32[384]{0:T(512)S(1)} %get-tuple-element.3, f32[384]{0:T(512)S(1)} %get-tuple-element.4, f32[384]{0:T(512)S(1)} %get-tuple-element.5, ...), kind=kLoop, calls=%fused_computation.33 | loop fusion | flops 24379392 | bytes 49592832 | tf_op jit(solution)/shard_map/convert_element_type | solution.py:59
  67.1 38.4 %all-gather.6.cloned.1.call-done = bf16[8,120,2048]{2,1,0:T(8,128)(2,1)} async-done(((bf16[8,120,512]{2,1,0:T(8,128)(2,1)}), bf16[8,120,2048]{2,1,0:T(8,128)(2,1)}) %all-gather.6.cloned.1.call-update) | async-done | bytes 3932176 | tf_op jit(solution)/shard_map/all_gather | solution.py:97
  105.4 4.5 %fusion.15 = f32[960,512]{1,0:T(8,128)S(1)} fusion(bf16[960,2048]{1,0:T(8,128)(2,1)} %bitcast.36, bf16[1,2048,512]{2,1,0:T(8,128)(2,1)S(1)} %copy-done), kind=kOutput, calls=%fused_computation.19 | convolution fusion | flops 2013265920 | bytes 7995392 | tf_op jit(solution)/shard_map/dot_general | solution.py:101
  109.9 3.6 %multiply_convert_fusion = bf16[960,512]{1,0:T(8,128)(2,1)} fusion(f32[960,512]{1,0:T(8,128)S(1)} %fusion.15, bf16[960,2048]{1,0:T(8,128)(2,1)S(1)} %bitcast.37, bf16[1,2048,512]{2,1,0:T(8,128)(2,1)S(1)} %copy-done.8), kind=kOutput, calls=%fused_computation.23 | convolution fusion | flops 2018181120 | bytes 8978432 | tf_op jit(solution)/shard_map/dot_general | solution.py:102
  113.7 37.3 %all-gather.4.cloned.1.call-done = bf16[1024,1536]{1,0:T(8,128)(2,1)} async-done(((bf16[1024,384]{1,0:T(8,128)(2,1)}), bf16[1024,1536]{1,0:T(8,128)(2,1)}) %all-gather.4.cloned.1.call-update) | async-done | bytes 3145744 | tf_op jit(solution)/shard_map/all_gather | solution.py:60
  151.0 2.4 convert_reduce_fusion
  153.4 50.3 %all-gather.8.cloned.1.call-done = bf16[960,2048]{1,0:T(8,128)(2,1)} async-done(((bf16[960,512]{1,0:T(8,128)(2,1)}), bf16[960,2048]{1,0:T(8,128)(2,1)}) %all-gather.8.cloned.1.call-update) | async-done | bytes 3932176 | tf_op jit(solution)/shard_map/all_gather | solution.py:19
  203.7 5.9 %fusion.60 = bf16[960,512]{1,0:T(8,128)(2,1)} fusion(bf16[960,2048]{1,0:T(8,128)(2,1)} %all-gather.8.cloned.1.call-done, bf16[1,2048,512]{2,1,0:T(8,128)(2,1)} %param.25), kind=kOutput, calls=%fused_computation.96 | convolution fusion | flops 2013757440 | bytes 7012352 | tf_op jit(solution)/shard_map/dot_general | solution.py:18
  209.6 4.6 %all-to-all-start.1 = ((bf16[8,120,512]{2,1,0:T(8,128)(2,1)}), bf16[8,120,512]{2,1,0:T(8,128)(2,1)S(1)}, u32[]{:S(2)}, u32[]{:S(2)}) async-start(bf16[8,120,512]{2,1,0:T(8,128)(2,1)} %bitcast.33), calls=%async_computation.1 | async-start | bytes 1966080 | tf_op jit(solution)/shard_map/all_to_all | solution.py:29
  214.3 3.0 %fusion.2 = f32[1024]{0:T(1024)S(1)} fusion(bf16[1024,1536]{1,0:T(8,128)(2,1)} %all-gather.4.cloned.1.call-done, f32[1024]{0:T(1024)S(1)} %broadcast_multiply_fusion.1), kind=kLoop, calls=%fused_computation.7 | loop fusion | flops 6290432 | bytes 3153920 | tf_op jit(solution)/shard_map/reduce_sum | solution.py:62
  217.3 5.2 %fusion.57 = bf16[1024,512]{1,0:T(8,128)(2,1)} fusion(bf16[1536,512]{1,0:T(8,128)(2,1)} %param.18, bf16[1024,1536]{1,0:T(8,128)(2,1)S(1)} %copy-done.1, f32[1536]{0:T(1024)S(1)} %copy-done.9, f32[1536]{0:T(1024)S(1)} %copy-done.10, f32[1024]{0:T(1024)S(1)} %add_rsqrt_fusion, f32[1024]{0:T(1024)S(1)} %broadcast_multiply_fusion.1), kind=kOutput, calls=%fused_computation.95 | convolution fusion | flops 1626865664 | bytes 5787648 | tf_op jit(solution)/shard_map/dot_general | solution.py:67
  222.5 16.9 %all-to-all-done.1 = bf16[8,120,512]{2,1,0:T(8,128)(2,1)S(1)} async-done(((bf16[8,120,512]{2,1,0:T(8,128)(2,1)}), bf16[8,120,512]{2,1,0:T(8,128)(2,1)S(1)}, u32[]{:S(2)}, u32[]{:S(2)}) %all-to-all-start.1) | async-done | bytes 983072 | tf_op jit(solution)/shard_map/all_to_all | solution.py:29
  239.4 3.3 %gather_fusion.1 = bf16[768,512]{1,0:T(8,128)(2,1)} fusion(bf16[960,512]{1,0:T(8,128)(2,1)S(1)} %bitcast.31, s32[1024]{0:T(1024)S(1)} %pad_clamp_fusion), kind=kCustom, calls=%fused_computation.1 | custom fusion | bytes 1575936 | tf_op jit(solution)/shard_map/gather | solution.py:104
  242.7 2.6 %reshape.98 = f32[192,4,512]{2,1,0:T(4,128)} reshape(bf16[768,512]{1,0:T(8,128)(2,1)} %gather_fusion.1) | data formatting | bytes 2359296 | tf_op jit(solution)/shard_map/convert_element_type | solution.py:105
  245.3 3.1 %multiply_reduce_fusion = bf16[192,512]{1,0:T(8,128)(2,1)} fusion(f32[192,4,512]{2,1,0:T(4,128)} %reshape.98, f32[192,4]{1,0:T(8,128)S(1)} %copy.23), kind=kLoop, calls=%fused_computation.93 | loop fusion | flops 688128 | bytes 1772544 | tf_op jit(solution)/shard_map/reduce_sum | solution.py:106
  (49 shorter events, 1.3 us)
Async XLA Ops:
  7.2 98.3 %copy-start = (bf16[1,2048,512]{2,1,0:T(8,128)(2,1)S(1)}, bf16[1,2048,512]{2,1,0:T(8,128)(2,1)}, u32[]{:S(2)}) copy-start(bf16[1,2048,512]{2,1,0:T(8,128)(2,1)} %param.23) | copy-start | bytes 6291460
  7.2 9.2 %copy-start.2 = (bf16[192,2048]{1,0:T(8,128)(2,1)S(1)}, bf16[192,2048]{1,0:T(8,128)(2,1)}, u32[]{:S(2)}) copy-start(bf16[192,2048]{1,0:T(8,128)(2,1)} %param.19) | copy-start | bytes 2359300
  7.2 9.6 %copy-start.5 = (f32[2048]{0:T(1024)S(1)}, f32[2048]{0:T(1024)}, u32[]{:S(2)}) copy-start(f32[2048]{0:T(1024)} %param.20) | copy-start | bytes 24580
  7.2 98.2 %all-gather.6.cloned.1.call-start = ((), (), s32[]{:S(2)}) async-start(), calls=%async_computation.3 | async-start | bytes 4915200 | tf_op jit(solution)/shard_map/all_gather | solution.py:97
  24.5 31.6 %copy-start.3 = (bf16[1024,384]{1,0:T(8,128)(2,1)S(1)}, bf16[1024,384]{1,0:T(8,128)(2,1)}, u32[]{:S(2)}) copy-start(bf16[1024,384]{1,0:T(8,128)(2,1)} %param.14) | copy-start | bytes 2359300
  56.0 3.2 %copy-start.4 = (f32[31,384]{1,0:T(8,128)S(1)}, f32[31,384]{1,0:T(8,128)}, u32[]{:S(2)}) copy-start(f32[31,384]{1,0:T(8,128)} %param.15) | copy-start | bytes 142852
  56.1 94.9 %all-gather.4.cloned.1.call-start = ((), (), s32[]{:S(2)}) async-start(), calls=%async_computation.2 | async-start | bytes 3932160 | tf_op jit(solution)/shard_map/all_gather | solution.py:60
  57.7 2.3 collective-permute-start
  67.0 136.7 %all-gather.8.cloned.1.call-start = ((), (), s32[]{:S(2)}) async-start(), calls=%async_computation.4 | async-start | bytes 4915200 | tf_op jit(solution)/shard_map/all_gather | solution.py:19
  105.4 4.5 %copy-start.7 = (bf16[8,120,2048]{2,1,0:T(8,128)(2,1)S(1)}, bf16[8,120,2048]{2,1,0:T(8,128)(2,1)}, u32[]{:S(2)}) copy-start(bf16[8,120,2048]{2,1,0:T(8,128)(2,1)} %all-gather.6.cloned.1.call-done) | copy-start | bytes 11796484
  105.4 4.5 %copy-start.8 = (bf16[1,2048,512]{2,1,0:T(8,128)(2,1)S(1)}, bf16[1,2048,512]{2,1,0:T(8,128)(2,1)}, u32[]{:S(2)}) copy-start(bf16[1,2048,512]{2,1,0:T(8,128)(2,1)} %param.24) | copy-start | bytes 6291460
  109.9 3.6 %copy-start.6 = (f32[192,4]{0,1:T(4,128)S(1)}, f32[192,4]{0,1:T(4,128)}, u32[]{:S(2)}) copy-start(f32[192,4]{0,1:T(4,128)} %param.22) | copy-start | bytes 9220
  209.6 29.8 %all-to-all-start.1 = ((bf16[8,120,512]{2,1,0:T(8,128)(2,1)}), bf16[8,120,512]{2,1,0:T(8,128)(2,1)S(1)}, u32[]{:S(2)}, u32[]{:S(2)}) async-start(bf16[8,120,512]{2,1,0:T(8,128)(2,1)} %bitcast.33), calls=%async_computation.1 | async-start | bytes 1966080 | tf_op jit(solution)/shard_map/all_to_all | solution.py:29
  214.2 3.0 %copy-start.1 = (bf16[1024,1536]{1,0:T(8,128)(2,1)S(1)}, bf16[1024,1536]{1,0:T(8,128)(2,1)}, u32[]{:S(2)}) copy-start(bf16[1024,1536]{1,0:T(8,128)(2,1)} %all-gather.4.cloned.1.call-done) | copy-start | bytes 9437188
  214.2 3.0 %copy-start.9 = (f32[1536]{0:T(1024)S(1)}, f32[1536]{0:T(1024)}, u32[]{:S(2)}) copy-start(f32[1536]{0:T(1024)} %param.17) | copy-start | bytes 18436
  214.2 3.0 %copy-start.10 = (f32[1536]{0:T(1024)S(1)}, f32[1536]{0:T(1024)}, u32[]{:S(2)}) copy-start(f32[1536]{0:T(1024)} %param.16) | copy-start | bytes 18436
Sparse Core Ops, SparseCore 0:
  56.2 49.1 all-gather.5
  107.2 43.6 all-gather.3
  153.4 50.2 all-gather.7
where the time goes:
time: 255 us
  waiting for transfers between devices  144 us (56%)
  blocking collectives  31.5 us (12%)
  other arithmetic  21.9 us (9%)
  matrix products  19.1 us (7%)
  local copies, waits for them, and re-layouts  18.6 us (7%)
  between operations  14 us (5%)
  starting transfers between devices  6.19 us (2%)
    all_gather x1, waiting for transfers between devices, expert_tail(): lax.all_gather(activation, 'tp', axis=1, tiled=True)  50.3 us
    all_gather x1, waiting for transfers between devices, body(): portion = lax.all_gather(arrived, 'tp', axis=2, tiled=True)  38.4 us
    all_gather x1, waiting for transfers between devices, body(): lax.all_gather(convolved, 'tp', axis=1, tiled=True).astype(jnp.float32)  37.3 us
    all_to_all x1, blocking collectives, body(): lax.all_to_all(columns, 'ep', split_axis=0, concat_axis=0, tiled=True)  31.5 us
    all_to_all x1, waiting for transfers between devices, finish(): lax.all_to_all(outcome, 'ep', split_axis=0, concat_axis=0, tiled=True)  16.9 us
    convert_element_type x1, other arithmetic, body(): convolved = running.astype(jnp.bfloat16)  6.79 us
    dot_general x1, matrix products, expert_tail(): jnp.dot(lax.all_gather(activation, 'tp', axis=1, tiled=True), weights, pr...  5.93 us
    gather x1, local copies, waits for them, and re-layouts, body(): outgoing = padded[slot_token].reshape(experts, capacity, model_width)  5.91 us
  transfers between devices with their start and end apart: 5, of which 5 were waited for; matrix products, arithmetic and copies ran while one was open for 11% of the time, Pallas kernels for 0%

commit v1 on v0

--- a/solution.py
+++ b/solution.py
@@ -94,7 +94,7 @@
     )
     arrived = lax.all_to_all(columns, "ep", split_axis=0, concat_axis=0, tiled=True)
     slot_total = arrived.shape[0] * arrived.shape[1]
-    portion = lax.all_gather(arrived, "tp", axis=2, tiled=True)
+    portion = jnp.concatenate(lax.all_gather(arrived, "tp"), axis=2)
     flattened = portion.reshape(slot_total, portion.shape[2])
     gate_part = gate_weight[0]
     up_part = up_weight[0]

time: 255 us -> 256 us (level)
  local copies, waits for them, and re-layouts: 18.6 us -> 25.1 us
  waiting for transfers between devices: 144 us -> 139 us
    reshape x0 -> x1, local copies, waits for them, and re-layouts: none -> 5.15 us  [body(): portion = jnp.concatenate(lax.all_gather(arrived, 'tp'), axis=2)]
    all_gather x1, waiting for transfers between devices: 37.3 us -> 33.1 us  [body(): lax.all_gather(convolved, 'tp', axis=1, tiled=True).astype(jnp.float32)]
  transfers between devices with their start and end apart: 5 -> 5, of which waited for: 5 -> 5; matrix products, arithmetic and copies ran while one was open for 11% -> 12% of each run, Pallas kernels for 0% -> 0%
where the time goes in v1:
time: 256 us; the launch traced here: 255 us
  waiting for transfers between devices  139 us (54%)
  blocking collectives  31.5 us (12%)
  local copies, waits for them, and re-layouts  25.1 us (10%)
  other arithmetic  21.9 us (9%)
  matrix products  16.8 us (7%)
  between operations  14 us (5%)
  starting transfers between devices  6.38 us (2%)
    all_gather x1, waiting for transfers between devices, expert_tail(): lax.all_gather(activation, 'tp', axis=1, tiled=True)  50.3 us
    all_gather x1, waiting for transfers between devices, body(): portion = jnp.concatenate(lax.all_gather(arrived, 'tp'), axis=2)  38.3 us
    all_gather x1, waiting for transfers between devices, body(): lax.all_gather(convolved, 'tp', axis=1, tiled=True).astype(jnp.float32)  33.1 us
    all_to_all x1, blocking collectives, body(): lax.all_to_all(columns, 'ep', split_axis=0, concat_axis=0, tiled=True)  31.5 us
    all_to_all x1, waiting for transfers between devices, finish(): lax.all_to_all(outcome, 'ep', split_axis=0, concat_axis=0, tiled=True)  16.9 us
    convert_element_type x1, other arithmetic, body(): convolved = running.astype(jnp.bfloat16)  6.79 us
    dot_general x1, matrix products, expert_tail(): jnp.dot(lax.all_gather(activation, 'tp', axis=1, tiled=True), weights, pr...  5.93 us
    gather x1, local copies, waits for them, and re-layouts, body(): outgoing = padded[slot_token].reshape(experts, capacity, model_width)  5.91 us
  transfers between devices with their start and end apart: 5, of which 5 were waited for; matrix products, arithmetic and copies ran while one was open for 12% of the time, Pallas kernels for 0%

profile of v1, /device:TPU:0, one launch (start us, length us, event | category | flops | bytes accessed | tf_op | source)
XLA Modules:
  0.0 255.1 jit_solution(5988340318084474093)
XLA Ops:
  7.2 0.9 copy.32
  8.4 0.7 broadcast_multiply_fusion
  9.1 1.7 reduce-window.6
  11.7 3.4 %scatter_custom_fusion = s32[960]{0:T(1024)S(1)} fusion(s32[768]{0:T(1024)S(1)} %fusion.69, s32[768]{0:T(1024)S(1)} %add_select_fusion, s32[]{:T(128)} %constant.28.clone.1), kind=kCustom, calls=%fused_computation.118 | custom fusion | bytes 3844 | tf_op jit(solution)/shard_map/scatter | solution.py:87
  15.1 1.3 convert_reduce_fusion.1
  16.4 0.4 fusion.23
  16.8 0.4 fusion.25
  17.3 5.9 %gather_fusion = bf16[960,2048]{1,0:T(8,128)(2,1)} fusion(bf16[193,2048]{1,0:T(8,128)(2,1)S(1)} %concatenate.7, s32[1024]{0:T(1024)S(1)} %pad_clamp_fusion.1), kind=kCustom, calls=%fused_computation | custom fusion | bytes 7868160 | tf_op jit(solution)/shard_map/gather | solution.py:90
  23.2 1.3 constant_dynamic-slice_fusion
  24.5 31.5 %all_to_all.10 = bf16[8,120,512]{2,1,0:T(8,128)(2,1)} all-to-all(bf16[8,120,512]{2,1,0:T(8,128)(2,1)S(1)} %constant_dynamic-slice_fusion), channel_id=1, replica_groups=mesh['ep'=8,'tp'=4] {'ep'}, dimensions={0} | all-to-all | bytes 1966080 | tf_op jit(solution)/shard_map/all_to_all | solution.py:95
  56.1 1.6 multiply_convert_fusion.1
  57.7 1.5 collective-permute-start
  59.4 0.6 collective-permute-done
  60.0 0.2 maximum_convert_fusion
  60.2 6.8 %fusion.27 = bf16[1024,384]{1,0:T(8,128)(2,1)} fusion(f32[1054,384]{1,0:T(8,128)S(1)} %maximum_convert_fusion, f32[384]{0:T(512)S(1)} %get-tuple-element.31, f32[384]{0:T(512)S(1)} %get-tuple-element.32, f32[384]{0:T(512)S(1)} %get-tuple-element.3, f32[384]{0:T(512)S(1)} %get-tuple-element.4, f32[384]{0:T(512)S(1)} %get-tuple-element.5, ...), kind=kLoop, calls=%fused_computation.33 | loop fusion | flops 24379392 | bytes 49592832 | tf_op jit(solution)/shard_map/convert_element_type | solution.py:59
  67.0 0.2 all-gather.7.cloned.1.call-start
  67.2 38.3 %all-gather.9.cloned.1.call-done = bf16[32,120,512]{2,1,0:T(8,128)(2,1)} async-done(((bf16[8,120,512]{2,1,0:T(8,128)(2,1)}), bf16[32,120,512]{2,1,0:T(8,128)(2,1)}) %all-gather.9.cloned.1.call-update) | async-done | bytes 3932176 | tf_op jit(solution)/shard_map/all_gather | solution.py:97
  105.6 5.1 %copy.36 = bf16[8,120,4,512]{3,2,1,0:T(4,128)(2,1)S(1)} copy(bf16[8,120,4,512]{3,1,0,2:T(8,128)(2,1)} %bitcast.39) | data formatting | bytes 7864320 | tf_op jit(solution)/shard_map/reshape | solution.py:97
  110.7 1.3 copy.38
  112.0 2.2 fusion.15
  114.2 3.6 %multiply_convert_fusion = bf16[960,512]{1,0:T(8,128)(2,1)} fusion(f32[960,512]{1,0:T(8,128)S(1)} %fusion.15, bf16[960,2048]{1,0:T(8,128)(2,1)S(1)} %bitcast.41, bf16[1,2048,512]{2,1,0:T(8,128)(2,1)S(1)} %copy-done.7), kind=kOutput, calls=%fused_computation.23 | convolution fusion | flops 2018181120 | bytes 8978432 | tf_op jit(solution)/shard_map/dot_general | solution.py:102
  118.0 33.1 %all-gather.5.cloned.1.call-done = bf16[1024,1536]{1,0:T(8,128)(2,1)} async-done(((bf16[1024,384]{1,0:T(8,128)(2,1)}), bf16[1024,1536]{1,0:T(8,128)(2,1)}) %all-gather.5.cloned.1.call-update) | async-done | bytes 3145744 | tf_op jit(solution)/shard_map/all_gather | solution.py:60
  151.1 2.4 convert_reduce_fusion
  153.5 50.3 %all-gather.7.cloned.1.call-done = bf16[960,2048]{1,0:T(8,128)(2,1)} async-done(((bf16[960,512]{1,0:T(8,128)(2,1)}), bf16[960,2048]{1,0:T(8,128)(2,1)}) %all-gather.7.cloned.1.call-update) | async-done | bytes 3932176 | tf_op jit(solution)/shard_map/all_gather | solution.py:19
  203.8 5.9 %fusion.60 = bf16[960,512]{1,0:T(8,128)(2,1)} fusion(bf16[960,2048]{1,0:T(8,128)(2,1)} %all-gather.7.cloned.1.call-done, bf16[1,2048,512]{2,1,0:T(8,128)(2,1)} %param.25), kind=kOutput, calls=%fused_computation.96 | convolution fusion | flops 2013757440 | bytes 7012352 | tf_op jit(solution)/shard_map/dot_general | solution.py:18
  209.7 4.6 %all-to-all-start.1 = ((bf16[8,120,512]{2,1,0:T(8,128)(2,1)}), bf16[8,120,512]{2,1,0:T(8,128)(2,1)S(1)}, u32[]{:S(2)}, u32[]{:S(2)}) async-start(bf16[8,120,512]{2,1,0:T(8,128)(2,1)} %bitcast.42), calls=%async_computation.1 | async-start | bytes 1966080 | tf_op jit(solution)/shard_map/all_to_all | solution.py:29
  214.4 3.0 %fusion.2 = f32[1024]{0:T(1024)S(1)} fusion(bf16[1024,1536]{1,0:T(8,128)(2,1)} %all-gather.5.cloned.1.call-done, f32[1024]{0:T(1024)S(1)} %broadcast_multiply_fusion.1), kind=kLoop, calls=%fused_computation.7 | loop fusion | flops 6290432 | bytes 3153920 | tf_op jit(solution)/shard_map/reduce_sum | solution.py:62
  217.4 5.2 %fusion.57 = bf16[1024,512]{1,0:T(8,128)(2,1)} fusion(bf16[1536,512]{1,0:T(8,128)(2,1)} %param.18, bf16[1024,1536]{1,0:T(8,128)(2,1)S(1)} %copy-done.1, f32[1536]{0:T(1024)S(1)} %copy-done.8, f32[1536]{0:T(1024)S(1)} %copy-done.9, f32[1024]{0:T(1024)S(1)} %add_rsqrt_fusion, f32[1024]{0:T(1024)S(1)} %broadcast_multiply_fusion.1), kind=kOutput, calls=%fused_computation.95 | convolution fusion | flops 1626865664 | bytes 5787648 | tf_op jit(solution)/shard_map/dot_general | solution.py:67
  222.6 16.9 %all-to-all-done.1 = bf16[8,120,512]{2,1,0:T(8,128)(2,1)S(1)} async-done(((bf16[8,120,512]{2,1,0:T(8,128)(2,1)}), bf16[8,120,512]{2,1,0:T(8,128)(2,1)S(1)}, u32[]{:S(2)}, u32[]{:S(2)}) %all-to-all-start.1) | async-done | bytes 983072 | tf_op jit(solution)/shard_map/all_to_all | solution.py:29
  239.5 3.3 %gather_fusion.1 = bf16[768,512]{1,0:T(8,128)(2,1)} fusion(bf16[960,512]{1,0:T(8,128)(2,1)S(1)} %bitcast.36, s32[1024]{0:T(1024)S(1)} %pad_clamp_fusion), kind=kCustom, calls=%fused_computation.1 | custom fusion | bytes 1575936 | tf_op jit(solution)/shard_map/gather | solution.py:104
  242.9 2.6 %reshape.98 = f32[192,4,512]{2,1,0:T(4,128)} reshape(bf16[768,512]{1,0:T(8,128)(2,1)} %gather_fusion.1) | data formatting | bytes 2359296 | tf_op jit(solution)/shard_map/convert_element_type | solution.py:105
  245.4 3.1 %multiply_reduce_fusion = bf16[192,512]{1,0:T(8,128)(2,1)} fusion(f32[192,4,512]{2,1,0:T(4,128)} %reshape.98, f32[192,4]{1,0:T(8,128)S(1)} %copy.37), kind=kLoop, calls=%fused_computation.93 | loop fusion | flops 688128 | bytes 1772544 | tf_op jit(solution)/shard_map/reduce_sum | solution.py:106
  (49 shorter events, 1.6 us)
Async XLA Ops:
  7.2 104.9 %copy-start = (bf16[1,2048,512]{2,1,0:T(8,128)(2,1)S(1)}, bf16[1,2048,512]{2,1,0:T(8,128)(2,1)}, u32[]{:S(2)}) copy-start(bf16[1,2048,512]{2,1,0:T(8,128)(2,1)} %param.23) | copy-start | bytes 6291460
  7.2 9.2 %copy-start.2 = (bf16[192,2048]{1,0:T(8,128)(2,1)S(1)}, bf16[192,2048]{1,0:T(8,128)(2,1)}, u32[]{:S(2)}) copy-start(bf16[192,2048]{1,0:T(8,128)(2,1)} %param.19) | copy-start | bytes 2359300
  7.2 9.6 %copy-start.5 = (f32[2048]{0:T(1024)S(1)}, f32[2048]{0:T(1024)}, u32[]{:S(2)}) copy-start(f32[2048]{0:T(1024)} %param.20) | copy-start | bytes 24580
  7.2 98.4 %all-gather.9.cloned.1.call-start = ((), (), s32[]{:S(2)}) async-start(), calls=%async_computation.4 | async-start | bytes 4915200 | tf_op jit(solution)/shard_map/all_gather | solution.py:97
  24.5 31.6 %copy-start.3 = (bf16[1024,384]{1,0:T(8,128)(2,1)S(1)}, bf16[1024,384]{1,0:T(8,128)(2,1)}, u32[]{:S(2)}) copy-start(bf16[1024,384]{1,0:T(8,128)(2,1)} %param.14) | copy-start | bytes 2359300
  56.0 3.2 %copy-start.4 = (f32[31,384]{1,0:T(8,128)S(1)}, f32[31,384]{1,0:T(8,128)}, u32[]{:S(2)}) copy-start(f32[31,384]{1,0:T(8,128)} %param.15) | copy-start | bytes 142852
  56.1 95.0 %all-gather.5.cloned.1.call-start = ((), (), s32[]{:S(2)}) async-start(), calls=%async_computation.2 | async-start | bytes 3932160 | tf_op jit(solution)/shard_map/all_gather | solution.py:60
  57.7 2.3 collective-permute-start
  67.0 136.8 %all-gather.7.cloned.1.call-start = ((), (), s32[]{:S(2)}) async-start(), calls=%async_computation.3 | async-start | bytes 4915200 | tf_op jit(solution)/shard_map/all_gather | solution.py:19
  112.0 2.2 copy-start.7
  114.2 3.6 %copy-start.6 = (f32[192,4]{0,1:T(4,128)S(1)}, f32[192,4]{0,1:T(4,128)}, u32[]{:S(2)}) copy-start(f32[192,4]{0,1:T(4,128)} %param.22) | copy-start | bytes 9220
  209.7 29.8 %all-to-all-start.1 = ((bf16[8,120,512]{2,1,0:T(8,128)(2,1)}), bf16[8,120,512]{2,1,0:T(8,128)(2,1)S(1)}, u32[]{:S(2)}, u32[]{:S(2)}) async-start(bf16[8,120,512]{2,1,0:T(8,128)(2,1)} %bitcast.42), calls=%async_computation.1 | async-start | bytes 1966080 | tf_op jit(solution)/shard_map/all_to_all | solution.py:29
  214.4 3.0 %copy-start.1 = (bf16[1024,1536]{1,0:T(8,128)(2,1)S(1)}, bf16[1024,1536]{1,0:T(8,128)(2,1)}, u32[]{:S(2)}) copy-start(bf16[1024,1536]{1,0:T(8,128)(2,1)} %all-gather.5.cloned.1.call-done) | copy-start | bytes 9437188
  214.4 3.0 %copy-start.8 = (f32[1536]{0:T(1024)S(1)}, f32[1536]{0:T(1024)}, u32[]{:S(2)}) copy-start(f32[1536]{0:T(1024)} %param.17) | copy-start | bytes 18436
  214.4 3.0 %copy-start.9 = (f32[1536]{0:T(1024)S(1)}, f32[1536]{0:T(1024)}, u32[]{:S(2)}) copy-start(f32[1536]{0:T(1024)} %param.16) | copy-start | bytes 18436
Sparse Core Ops, SparseCore 0:
  56.2 49.3 all-gather.8
  107.4 43.6 all-gather.4
  153.5 50.2 all-gather.6
